TPU v7x, 32 devices: a whole 2x2x4 slice. The times are simulated.
32 devices in a mesh: fs: 8 (over z, x), tp: 4 (over y, core).
Axes of the slice: x: 2, y: 2, z: 4, core: 2. Of those that a mesh axis runs over, the one named last changes fastest.
Arguments:
- tokens: bfloat16 [1536, 2048], P('fs'), may hold values from -6 to 6
- norm_gain: float32 [2048], P('fs'), may hold values from 0.1 to 1.9
- expert_gate: float32 [16, 2048, 1024], P(None, 'fs', 'tp'), may hold values from -0.125 to 0.125
- expert_up: float32 [16, 2048, 1024], P(None, 'fs', 'tp'), may hold values from -0.125 to 0.125
- expert_down: float32 [16, 1024, 2048], P(None, 'fs', 'tp'), may hold values from -0.1875 to 0.1875
- shared_gate: float32 [2048, 1024], P('fs', 'tp'), may hold values from -0.125 to 0.125
- shared_up: float32 [2048, 1024], P('fs', 'tp'), may hold values from -0.125 to 0.125
- shared_down: float32 [1024, 2048], P('fs', 'tp'), may hold values from -0.1875 to 0.1875
- expert_ids: int32 [1536, 8], P('fs'), may hold values from 0 to 15, all different within a row; in each aligned block of 192 rows (0 to 191, 192 to 383, ...) at most 192 rows name the same one
- route_weights: float32 [1536, 8], P('fs'), may hold values from 0.25 to 1
Outputs:
- gate_ready: bfloat16 [16, 2048, 1024], P('fs', None, 'tp')
- up_ready: bfloat16 [16, 2048, 1024], P('fs', None, 'tp')
- down_ready: bfloat16 [16, 1024, 2048], P('fs', None, 'tp')
- shared_gate_ready: bfloat16 [2048, 1024], P(None, 'tp')
- shared_up_ready: bfloat16 [2048, 1024], P(None, 'tp')
- shared_down_ready: bfloat16 [1024, 2048], P(None, 'tp')
- mixed: bfloat16 [1536, 2048], P('fs', 'tp')
Inputs may be any that keep to these rules, and one draw needn't show every extreme that they name: `expert_ids`: each row names 8 different experts. Among the 192 rows of one index of fs no expert is named more than 192 times, and in every draw some expert is named exactly 192 times there.
All inputs are finite; a program needn't handle non-finite values.
Results may differ from a plain program's by a relative error of at most 0.0085.
Values may be sent and summed in bfloat16 or wider, within the bound.
A program may use at most 128 MiB of HBM per device.

v0:
```python
import functools
import jax
import jax.numpy as jnp
from jax import lax
from jax.experimental import pallas as pl
from jax.experimental.pallas import tpu as pltpu
from jax.sharding import PartitionSpec as P

TOP_K = 8


EPS = 1e-06

MESH = pl.DeviceIdType.MESH
LANES = 128
VMEM_BYTES = 48 * 1024 * 1024


def flip(value, mask, extent):
    result, bit = 0, 1
    while bit < extent:
        digit = (value // bit) % 2
        result = result + bit * ((1 - digit) if mask & bit else digit)
        bit *= 2
    return result


def fused_kernel(
    groups,
    ranks,
    ext,
    gain,
    eg,
    eu,
    ed,
    sg,
    su,
    sd,
    rv_g,
    rv_u,
    rv_d,
    out_sg,
    out_su,
    out_sd,
    out_mixed,
    st_g,
    st_u,
    st_d,
    sb_g,
    sb_u,
    sb_d,
    sh,
    tok,
    hid,
    shid,
    xs,
    xr,
    zs,
    zr,
    own_out,
    load_sem,
    loc_sem,
    own_sem,
    a2a_send,
    a2a_recv,
    tok_send,
    tok_recv,
    tok_tsend,
    tok_trecv,
    sh_send,
    sh_recv,
    hid_csend,
    hid_ysend,
    hid_fsend,
    hid_recv,
    shid_send,
    shid_recv,
    x_send,
    x_recv,
    z_send,
    z_recv,
    shout_sem,
):
    nx = 2
    nz = groups // nx
    me = lax.axis_index("fs")
    tp = lax.axis_index("tp")
    z, x = me // nx, me % nx
    partner = flip(tp, 1, ranks)
    across = flip(tp, 2, ranks)
    per = eg.shape[0] // groups
    experts = eg.shape[0]
    rows_w = eg.shape[1]
    rows_d = ed.shape[1]
    tok_count = ext.shape[0]
    width = st_d.shape[2] * ranks
    share = tok_count // ranks
    hcols = eg.shape[2]
    dcols = ed.shape[2]
    hw = dcols // 2

    loads = [
        pltpu.make_async_copy(a, b, load_sem.at[i])
        for i, (a, b) in enumerate(((eg, st_g), (eu, st_u), (ed, st_d)))
    ]
    for load in loads:
        load.start()
    own_tok = pltpu.make_async_copy(ext, tok.at[me], loc_sem)
    own_tok.start()

    barrier = pltpu.get_barrier_semaphore()
    for o in range(1, groups):
        pl.semaphore_signal(
            barrier, inc=1, device_id={"fs": flip(me, o, groups)}, device_id_type=MESH
        )
    for o in range(1, ranks):
        pl.semaphore_signal(
            barrier, inc=1, device_id={"tp": flip(tp, o, ranks)}, device_id_type=MESH
        )
    pl.semaphore_wait(barrier, groups + ranks - 2)

    mine = pl.ds(tp * share, share)
    theirs = pl.ds(across * share, share)

    def fs_copy(src, dst, send, recv, target):
        return pltpu.make_async_remote_copy(
            src_ref=src,
            dst_ref=dst,
            send_sem=send,
            recv_sem=recv,
            device_id={"fs": target},
            device_id_type=MESH,
        )

    def tp_copy(src, dst, send, recv, target):
        return pltpu.make_async_remote_copy(
            src_ref=src,
            dst_ref=dst,
            send_sem=send,
            recv_sem=recv,
            device_id={"tp": target},
            device_id_type=MESH,
        )

    def tok_copy(block, slot, target, own=False):
        src = ext.at[mine] if own else tok.at[block, mine]
        return fs_copy(src, tok.at[block, mine], tok_send.at[slot], tok_recv.at[block], target)

    def sh_copy(block, slot, target, own=False):
        return fs_copy(sh.at[block], sh.at[block], sh_send.at[slot], sh_recv.at[block], target)

    def gather_moves(copy, recv_copy, step, act):
        other = 1 - x
        if step == 0:

            @pl.when(z + 1 < nz)
            def _():
                act(copy(me, 0, me + nx, True))

            @pl.when(z >= 1)
            def _():
                act(copy(me, 1, me - nx, True))

            act(copy(me, 2, z * nx + other, True))
            return

        @pl.when(z >= step)
        def _():
            block = me - step * nx
            recv_copy(block)

            @pl.when(z + 1 < nz)
            def _():
                act(copy(block, 4 * step - 1, me + nx))

            act(copy(block, 4 * step, z * nx + other))

        @pl.when(z + step < nz)
        def _():
            block = me + step * nx
            recv_copy(block)

            @pl.when(z >= 1)
            def _():
                act(copy(block, 4 * step + 1, me - nx))

            act(copy(block, 4 * step + 2, z * nx + other))

    def start(c):
        c.start()

    def wait_send(c):
        c.wait_send()

    def nothing(block):
        pass

    def tok_arrive(block):
        tok_copy(block, 0, me).wait_recv()
        tok_share(0, block).start()
        tok_share(1, block).start()

    def tok_share(kind, block):
        rows = theirs if kind == 2 else mine
        return tp_copy(
            tok.at[block, rows],
            tok.at[block, rows],
            tok_tsend.at[kind, block],
            tok_trecv.at[kind, block],
            across if kind == 1 else partner,
        )

    def sh_arrive(block):
        sh_copy(block, 0, me).wait_recv()

    gather_moves(tok_copy, nothing, 0, start)

    column = gain[...]
    sh[me, 0] = (sg[...] * column).astype(jnp.bfloat16)
    sh[me, 1] = (su[...] * column).astype(jnp.bfloat16)
    sh[me, 2, 0:rows_d] = sd[:, 0:hw].astype(jnp.bfloat16)
    sh[me, 2, rows_d : 2 * rows_d] = sd[:, hw:dcols].astype(jnp.bfloat16)

    def cast(stage, sendbuf, scaled):
        @pl.loop(0, experts)
        def _(e):
            value = stage[e]
            if scaled:
                value = value * gain[...]
            sendbuf[e] = value.astype(jnp.bfloat16)

    order = [o for o in (7, 5, 6, 4, 3, 2, 1) if o < groups]
    order = order + [o for o in range(1, groups) if o not in order]

    def a2a_ends(index, piece, owner_at, row_at):
        if index < 2:
            sendbuf, recvbuf = ((sb_g, rv_g), (sb_u, rv_u))[index]
            return (
                sendbuf.at[owner_at * per + piece],
                recvbuf.at[piece, pl.ds(row_at * rows_w, rows_w), :],
            )
        columns = pl.ds(piece * hw, hw)
        return (
            sb_d.at[pl.ds(owner_at * per, per), :, columns],
            rv_d.at[:, pl.ds(row_at * rows_d, rows_d), columns],
        )

    def pieces(index):
        return per if index < 2 else 2

    def a2a_copy(index, piece, o):
        target = flip(me, o, groups)
        src, dst = a2a_ends(index, piece, target, me)
        return fs_copy(
            src, dst, a2a_send.at[index, piece, o], a2a_recv.at[index, piece, o], target
        )

    def a2a_own(index, piece):
        src, dst = a2a_ends(index, piece, me, me)
        return pltpu.make_async_copy(src, dst, own_sem.at[index, piece])

    def a2a_start(index, piece):
        for o in order:
            a2a_copy(index, piece, o).start()
        a2a_own(index, piece).start()

    def a2a_arrive(index, piece):
        for o in order:
            a2a_copy(index, piece, o).wait_recv()
        a2a_own(index, piece).wait()

    loads[0].wait()
    cast(st_g, sb_g, True)
    gather_moves(sh_copy, nothing, 0, start)
    gather_moves(tok_copy, tok_arrive, 1, start)
    a2a_start(0, 0)
    loads[1].wait()
    cast(st_u, sb_u, True)
    for step in range(2, nz):
        gather_moves(tok_copy, tok_arrive, step, start)
        if step == 2:
            a2a_start(1, 0)
            loads[2].wait()
            cast(st_d, sb_d, False)
            gather_moves(sh_copy, sh_arrive, 1, start)

    for zz in range(nz):
        tok_arrive(zz * nx + (1 - x))
    own_tok.wait()
    for o in range(1, groups):
        tok_share(1, flip(me, o, groups)).wait_recv()
        tok_share(2, flip(me, o, groups)).start()
    for piece in range(1, per):
        a2a_start(0, piece)
        a2a_start(1, piece)
    for step in range(2, nz - 1):
        gather_moves(sh_copy, sh_arrive, step, start)

    def sh_out(block, part):
        src_dst = (
            (sh.at[block, 0], out_sg.at[pl.ds(block * rows_w, rows_w), :]),
            (sh.at[block, 1], out_su.at[pl.ds(block * rows_w, rows_w), :]),
            (sh.at[block, 2, pl.ds(0, rows_d)], out_sd.at[pl.ds(block * rows_d, rows_d), pl.ds(0, hw)]),
            (sh.at[block, 2, pl.ds(rows_d, rows_d)], out_sd.at[pl.ds(block * rows_d, rows_d), pl.ds(hw, hw)]),
        )[part]
        return pltpu.make_async_copy(*src_dst, shout_sem.at[block, part])

    features = groups * rows_w

    def shared_half(part):
        total = jnp.zeros((tok_count, hcols), jnp.float32)
        for block in range(groups):
            total = total + jnp.dot(
                ext[:, block * rows_w : (block + 1) * rows_w],
                sh[block, part],
                preferred_element_type=jnp.float32,
            )
        return total

    def shared_hidden():
        for zz in range(nz):
            sh_arrive(zz * nx + (1 - x))
        for block in range(groups):
            for part in range(4):
                sh_out(block, part).start()
        first = shared_half(0)
        second = shared_half(1)
        shid[tp] = (jax.nn.silu(first) * second).astype(jnp.bfloat16)

    def shid_copy(o):
        return tp_copy(
            shid.at[tp], shid.at[tp], shid_send.at[o], shid_recv.at[o], flip(tp, o, ranks)
        )

    for o in range(1, groups):
        tok_share(0, flip(me, o, groups)).wait_recv()
        tok_share(2, flip(me, o, groups)).wait_recv()

    def hid_core(e, block):
        return tp_copy(
            hid.at[tp, block, e],
            hid.at[tp, block, e],
            hid_csend.at[e, block],
            hid_recv.at[0, e, block],
            partner,
        )

    def hid_across(e, block):
        return tp_copy(
            hid.at[tp, block, e],
            hid.at[tp, block, e],
            hid_ysend.at[e, block],
            hid_recv.at[1, e, block],
            across,
        )

    def hid_forward(e, block):
        return tp_copy(
            hid.at[across, block, e],
            hid.at[across, block, e],
            hid_fsend.at[e, block],
            hid_recv.at[2, e, block],
            partner,
        )

    def turn(o):
        return (me + o) % groups

    def shared_out():
        for o in range(1, ranks):
            shid_copy(o).wait_recv()
        for part in range(2):
            total = jnp.zeros((tok_count, hw), jnp.float32)
            for block in range(groups):
                at = block * rows_d
                total = total + jnp.dot(
                    shid[at // hcols, :, at % hcols : at % hcols + rows_d],
                    sh[block, 2, part * rows_d : (part + 1) * rows_d],
                    preferred_element_type=jnp.float32,
                )
            own_out[:, part * hw : (part + 1) * hw] = total

    for e in range(per):
        a2a_arrive(0, e)
        a2a_arrive(1, e)
        if e == 0:
            a2a_start(2, 0)
            a2a_start(2, 1)

        @pl.loop(0, groups)
        def _(o):
            block = turn(o + 1)
            rows = tok[block, :, 0:features]
            first = jnp.dot(rows, rv_g[e], preferred_element_type=jnp.float32)
            second = jnp.dot(rows, rv_u[e], preferred_element_type=jnp.float32)
            hid[tp, block, e] = (jax.nn.silu(first) * second).astype(jnp.bfloat16)

            @pl.when(o >= 1)
            def _():
                before = turn(o)
                hid_across(e, before).start()
                hid_core(e, before).start()

        if e > 0:
            hid_across(e - 1, turn(1)).wait_recv()
            hid_forward(e - 1, turn(1)).start()
        if e == per - 1:
            shared_hidden()
        hid_across(e, me).start()
        hid_core(e, me).start()

        @pl.loop(0 if e == per - 1 else 1, groups)
        def _(o):
            block = turn(o + 1)
            hid_across(e, block).wait_recv()
            hid_forward(e, block).start()

        if e == 0:
            gather_moves(sh_copy, sh_arrive, nz - 1, start)
        if e == per - 1:
            for o in range(1, ranks):
                shid_copy(o).start()

    shared_out()

    @pl.loop(1, groups + 1)
    def _(o):
        block = turn(o)
        for e in range(per):
            hid_core(e, block).wait_recv()
            hid_forward(e, block).wait_recv()

    lanes = lax.broadcasted_iota(jnp.int32, (tok_count, LANES), 1)

    def block_out(block, half_at):
        table = tok[block, :, features : features + LANES].astype(jnp.float32)
        total = jnp.zeros((tok_count, hw), jnp.float32)
        for e in range(per):
            expert = me * per + e
            weight = jnp.sum(
                jnp.where(
                    (lanes == expert) | (lanes == expert + experts) | (lanes == expert + 2 * experts),
                    table,
                    0.0,
                ),
                axis=1,
                keepdims=True,
            )
            out = jnp.zeros((tok_count, hw), jnp.float32)
            for r in range(ranks):
                out = out + jnp.dot(
                    hid[r, block, e],
                    rv_d[e, r * hcols : (r + 1) * hcols, half_at * hw : (half_at + 1) * hw],
                    preferred_element_type=jnp.float32,
                )
            total = total + weight * out
        return total

    def x_copy(part, zz):
        return fs_copy(
            xs.at[part, zz],
            xr.at[part, zz],
            x_send.at[part, zz],
            x_recv.at[part, zz],
            z * nx + (1 - x),
        )

    def z_copy(part, j):
        zz = (z + j) % nz
        return fs_copy(
            zs.at[part, zz], zr.at[part, z], z_send.at[part, j], z_recv.at[part, j], zz * nx + x
        )

    def x_stage(part):
        @pl.loop(1, nz + 1)
        def _(j):
            zz = (z + j) % nz
            xs[part, zz] = block_out(zz * nx + (1 - x), part).astype(jnp.bfloat16)

            @pl.when(j >= 2)
            def _():
                x_copy(part, (z + j - 1) % nz).start()

    def z_stage(part):
        @pl.loop(1, nz + 1)
        def _(j):
            zz = (z + j) % nz
            total = block_out(zz * nx + x, part)

            @pl.when(j == 1)
            def _():
                x_copy(part, z).start()

            x_copy(part, zz).wait_recv()
            total = total + xr[part, zz].astype(jnp.float32)

            @pl.when(j < nz)
            def _():
                zs[part, zz] = total.astype(jnp.bfloat16)

            @pl.when(j == nz)
            def _():
                columns = slice(part * hw, (part + 1) * hw)
                own_out[:, columns] = own_out[:, columns] + total

            @pl.when(j >= 2)
            def _():
                z_copy(part, j - 1).start()

    for part in range(2):
        a2a_arrive(2, part)
        x_stage(part)
        z_stage(part)

    for part in range(2):
        columns = slice(part * hw, (part + 1) * hw)
        for j in range(1, nz):
            z_copy(part, j).wait_recv()
            own_out[:, columns] = own_out[:, columns] + zr[part, (z + nz - j) % nz].astype(jnp.float32)
        out_mixed[:, columns] = own_out[:, columns].astype(jnp.bfloat16)

    for part in range(2):
        for j in range(nz):
            x_copy(part, j).wait_send()
        for j in range(1, nz):
            z_copy(part, j).wait_send()
    for index in range(3):
        for piece in range(pieces(index)):
            for o in order:
                a2a_copy(index, piece, o).wait_send()
    for step in range(nz):
        gather_moves(tok_copy, nothing, step, wait_send)
        gather_moves(sh_copy, nothing, step, wait_send)
    for o in range(1, groups):
        for kind in range(3):
            tok_share(kind, flip(me, o, groups)).wait_send()
    for o in range(1, ranks):
        shid_copy(o).wait_send()

    @pl.loop(0, groups)
    def _(o):
        for e in range(per):
            hid_core(e, o).wait_send()
            hid_across(e, o).wait_send()
            hid_forward(e, o).wait_send()

    for block in range(groups):
        for part in range(4):
            sh_out(block, part).wait()


def dense_body(
    tokens,
    norm_gain,
    expert_gate,
    expert_up,
    expert_down,
    shared_gate,
    shared_up,
    shared_down,
    expert_ids,
    route_weights,
):
    groups, ranks = lax.axis_size("fs"), lax.axis_size("tp")
    experts, rows_w, hcols = expert_gate.shape
    rows_d, dcols = expert_down.shape[1:]
    per = experts // groups
    tok_count, features = tokens.shape
    wide = tokens.astype(jnp.float32)
    normed = (wide * lax.rsqrt(jnp.mean(wide * wide, axis=-1, keepdims=True) + EPS)).astype(
        jnp.bfloat16
    )
    named = expert_ids[:, :, None] == jnp.arange(experts, dtype=jnp.int32)[None, None, :]
    table = jnp.sum(jnp.where(named, route_weights[:, :, None], 0.0), axis=1)
    high = lax.reduce_precision(table, 8, 7)
    middle = lax.reduce_precision(table - high, 8, 7)
    low = table - high - middle
    pad = jnp.zeros((tok_count, LANES - 3 * experts), jnp.bfloat16)
    ext = jnp.concatenate(
        [normed] + [v.astype(jnp.bfloat16) for v in (high, middle, low)] + [pad], axis=1
    )
    total = features + LANES
    bf, f32 = jnp.bfloat16, jnp.float32
    dma = pltpu.SemaphoreType.DMA
    nz = groups // 2
    any_space = pl.BlockSpec(memory_space=pl.ANY)
    vmem = pl.BlockSpec(memory_space=pltpu.VMEM)
    hidden = hcols * ranks
    return pl.pallas_call(
        functools.partial(fused_kernel, groups, ranks),
        out_shape=(
            pltpu.VMEM((per, features, hcols), bf),
            pltpu.VMEM((per, features, hcols), bf),
            pltpu.VMEM((per, hidden, dcols), bf),
            pltpu.VMEM((features, hcols), bf),
            pltpu.VMEM((features, hcols), bf),
            pltpu.VMEM((hidden, dcols), bf),
            pltpu.VMEM((tok_count, dcols), bf),
        ),
        in_specs=[vmem, vmem, any_space, any_space, any_space, vmem, vmem, vmem],
        out_specs=(vmem,) * 7,
        scratch_shapes=[
            pltpu.VMEM((experts, rows_w, hcols), f32),
            pltpu.VMEM((experts, rows_w, hcols), f32),
            pltpu.VMEM((experts, rows_d, dcols), f32),
            pltpu.VMEM((experts, rows_w, hcols), bf),
            pltpu.VMEM((experts, rows_w, hcols), bf),
            pltpu.VMEM((experts, rows_d, dcols), bf),
            pltpu.VMEM((groups, 3, rows_w, hcols), bf),
            pltpu.VMEM((groups, tok_count, total), bf),
            pltpu.VMEM((ranks, groups, per, tok_count, hcols), bf),
            pltpu.VMEM((ranks, tok_count, hcols), bf),
            pltpu.VMEM((2, nz, tok_count, dcols // 2), bf),
            pltpu.VMEM((2, nz, tok_count, dcols // 2), bf),
            pltpu.VMEM((2, nz, tok_count, dcols // 2), bf),
            pltpu.VMEM((2, nz, tok_count, dcols // 2), bf),
            pltpu.VMEM((tok_count, dcols), f32),
            dma((3,)),
            dma,
            dma((3, max(per, 2))),
            dma((3, max(per, 2), groups)),
            dma((3, max(per, 2), groups)),
            dma((4 * nz,)),
            dma((groups,)),
            dma((3, groups)),
            dma((3, groups)),
            dma((4 * nz,)),
            dma((groups,)),
            dma((per, groups)),
            dma((per, groups)),
            dma((per, groups)),
            dma((3, per, groups)),
            dma((ranks,)),
            dma((ranks,)),
            dma((2, nz)),
            dma((2, nz)),
            dma((2, nz)),
            dma((2, nz)),
            dma((groups, 4)),
        ],
        compiler_params=pltpu.CompilerParams(
            collective_id=0, has_side_effects=True, vmem_limit_bytes=VMEM_BYTES
        ),
    )(
        ext,
        norm_gain[:, None],
        expert_gate,
        expert_up,
        expert_down,
        shared_gate,
        shared_up,
        shared_down,
    )


def expert_hidden(rows, gate_new, up_new):
    first = jnp.einsum("secn,enf->secf", rows, gate_new, preferred_element_type=jnp.float32)
    second = jnp.einsum("secn,enf->secf", rows, up_new, preferred_element_type=jnp.float32)
    return (jax.nn.silu(first) * second).astype(jnp.bfloat16)


def body(
    tokens,
    norm_gain,
    expert_gate,
    expert_up,
    expert_down,
    shared_gate,
    shared_up,
    shared_down,
    expert_ids,
    route_weights,
):
    groups = lax.axis_size("fs")
    experts = expert_gate.shape[0]
    per_group = experts // groups
    tok_count = tokens.shape[0]
    capacity = 2 * tok_count * TOP_K // experts
    ranks = lax.axis_size("tp")
    square = expert_down.shape[1] * expert_down.shape[2] == shared_gate.size
    if capacity >= tok_count and per_group >= 2 and groups >= 8 and groups & (groups - 1) == 0 and ranks == 4 and square:
        return dense_body(
            tokens,
            norm_gain,
            expert_gate,
            expert_up,
            expert_down,
            shared_gate,
            shared_up,
            shared_down,
            expert_ids,
            route_weights,
        )
    gate_local = (expert_gate * norm_gain[None, :, None]).astype(jnp.bfloat16)
    up_local = (expert_up * norm_gain[None, :, None]).astype(jnp.bfloat16)
    down_local = expert_down.astype(jnp.bfloat16)
    gate_local = gate_local.reshape((groups, per_group) + gate_local.shape[1:])
    up_local = up_local.reshape((groups, per_group) + up_local.shape[1:])
    down_local = down_local.reshape((groups, per_group) + down_local.shape[1:])
    shared_first_local = (shared_gate * norm_gain[:, None]).astype(jnp.bfloat16)
    shared_second_local = (shared_up * norm_gain[:, None]).astype(jnp.bfloat16)
    shared_third_local = shared_down.astype(jnp.bfloat16)
    gate_moved, up_moved, down_moved = (
        lax.all_to_all(gate_local, "fs", split_axis=0, concat_axis=2, tiled=True),
        lax.all_to_all(up_local, "fs", split_axis=0, concat_axis=2, tiled=True),
        lax.all_to_all(down_local, "fs", split_axis=0, concat_axis=2, tiled=True),
    )
    down_ready = down_moved[0]
    gate_ready = gate_moved[0]
    up_ready = up_moved[0]
    shared_gate_ready, shared_up_ready, shared_down_ready = (
        lax.all_gather(shared_first_local, "fs", axis=0, tiled=True),
        lax.all_gather(shared_second_local, "fs", axis=0, tiled=True),
        lax.all_gather(shared_third_local, "fs", axis=0, tiled=True),
    )
    wide = tokens.astype(jnp.float32)
    normed = (wide * lax.rsqrt(jnp.mean(wide * wide, axis=-1, keepdims=True) + EPS)).astype(
        jnp.bfloat16
    )
    chosen = expert_ids.reshape(-1)
    onehot = (chosen[:, None] == jnp.arange(experts, dtype=jnp.int32)[None, :]).astype(jnp.int32)
    ranks = jnp.sum(jnp.cumsum(onehot, axis=0) * onehot, axis=1) - 1
    owners = jnp.arange(tok_count * TOP_K, dtype=jnp.int32) // TOP_K
    slot_token = jnp.zeros((experts, capacity), jnp.int32).at[chosen, ranks].set(owners)
    outgoing = normed[slot_token.reshape(-1)].reshape(groups, per_group, capacity, normed.shape[1])
    share = capacity // lax.axis_size("tp")
    mine = lax.dynamic_slice_in_dim(outgoing, lax.axis_index("tp") * share, share, 2)
    arrived = lax.all_to_all(mine, "fs", split_axis=0, concat_axis=0, tiled=True)
    hidden = expert_hidden(lax.all_gather(arrived, "tp", axis=2, tiled=True), gate_ready, up_ready)
    shared_first = jnp.dot(normed, shared_gate_ready, preferred_element_type=jnp.float32)
    shared_second = jnp.dot(normed, shared_up_ready, preferred_element_type=jnp.float32)
    shared_hidden = (jax.nn.silu(shared_first) * shared_second).astype(jnp.bfloat16)[None, None]
    columns = down_ready.shape[2]
    routed_piece = lax.all_gather(hidden, "tp", axis=3, tiled=True)
    shared_piece = lax.all_gather(shared_hidden, "tp", axis=3, tiled=True)
    routed_total = jnp.einsum(
        "secf,efd->secd", routed_piece, down_ready, preferred_element_type=jnp.float32
    )
    shared_total = jnp.einsum(
        "abtf,fd->abtd", shared_piece, shared_down_ready, preferred_element_type=jnp.float32
    )
    returned = lax.all_to_all(
        routed_total.astype(jnp.bfloat16), "fs", split_axis=0, concat_axis=0, tiled=True
    )
    returned = returned.reshape(experts * capacity, columns)
    picked = (
        returned[chosen * capacity + ranks].astype(jnp.float32).reshape(tok_count, TOP_K, columns)
    )
    routed = jnp.sum(picked * route_weights[:, :, None], axis=1)
    mixed = (shared_total[0, 0] + routed).astype(jnp.bfloat16)
    return (
        gate_ready,
        up_ready,
        down_ready,
        shared_gate_ready,
        shared_up_ready,
        shared_down_ready,
        mixed,
    )


def solution(mesh):
    in_specs = (
        P("fs", None),
        P("fs"),
        P(None, "fs", "tp"),
        P(None, "fs", "tp"),
        P(None, "fs", "tp"),
        P("fs", "tp"),
        P("fs", "tp"),
        P("fs", "tp"),
        P("fs", None),
        P("fs", None),
    )
    out_specs = (
        P("fs", None, "tp"),
        P("fs", None, "tp"),
        P("fs", None, "tp"),
        P(None, "tp"),
        P(None, "tp"),
        P(None, "tp"),
        P("fs", "tp"),
    )
    return jax.shard_map(body, mesh=mesh, in_specs=in_specs, out_specs=out_specs, check_vma=False)
```

profile of v0, /device:TPU:0, one launch (start us, length us, event | category | flops | bytes accessed | tf_op | source)
XLA Modules:
  0.0 215.1 jit_solution(5555134775741975520)
XLA Ops:
  0.6 0.0 copy-start
  0.6 1.4 fusion
  2.1 0.7 select_reduce_fusion
  2.9 0.1 copy.27
  3.0 0.1 copy.26
  3.1 0.1 copy.25
  3.2 1.5 copy.28.gain
  4.7 0.0 copy-done
  4.7 0.2 fusion.1
  4.9 1.1 concatenate.3.ext
  6.0 201.6 %shard_map.153 = (bf16[2,2048,256]{2,1,0:T(8,128)(2,1)S(1)}, bf16[2,2048,256]{2,1,0:T(8,128)(2,1)S(1)}, bf16[2,1024,512]{2,1,0:T(8,128)(2,1)S(1)}, bf16[2048,256...) custom-call(bf16[192,2176]{1,0:T(8,128)(2,1)} %concatenate.3.ext, ...), custom_call_target="tpu_custom_call" | custom-call | tf_op jit(solution)/shard_map/pallas_call | solution.py:589
  207.6 1.3 copy.36
  208.9 0.7 copy.42
  209.6 1.0 copy.39
  210.6 1.0 copy.40
  211.5 1.0 copy.41
  212.5 1.3 copy.37
  213.8 1.3 copy.38
  (4 shorter events, 0.0 us)
Async XLA Ops:
  0.6 4.0 %copy-start = (bf16[192,2048]{1,0:T(8,128)(2,1)S(1)}, bf16[192,2048]{1,0:T(8,128)(2,1)}, u32[]{:S(2)}) copy-start(bf16[192,2048]{1,0:T(8,128)(2,1)} %param.10) | copy-start | bytes 2359300
where the time goes:
time: 215 us
  Pallas kernels  202 us (94%)
  local copies, waits for them, and re-layouts  10.4 us (5%)
  other arithmetic  2.42 us (1%)
    pallas_call x1, Pallas kernels, dense_body(): pl.pallas_call(functools.partial(fused_kernel, groups, ranks), out_shape=...  202 us
    unnamed x9, local copies, waits for them, and re-layouts  7.55 us

commit v1 on v0

v1 whole, which is shorter than its diff:
```python
import functools
import jax
import jax.numpy as jnp
from jax import lax
from jax.experimental import pallas as pl
from jax.experimental.pallas import tpu as pltpu
from jax.sharding import PartitionSpec as P

TOP_K = 8


EPS = 1e-06

MESH = pl.DeviceIdType.MESH
LANES = 128
VMEM_BYTES = 44 * 1024 * 1024
scope = jax.named_scope


def flip(value, mask, extent):
    result, bit = 0, 1
    while bit < extent:
        digit = (value // bit) % 2
        result = result + bit * ((1 - digit) if mask & bit else digit)
        bit *= 2
    return result


def fused_kernel(
    groups,
    ranks,
    tokens,
    gain,
    ids,
    weights,
    eg,
    eu,
    ed,
    sg,
    su,
    sd,
    rv_g,
    rv_u,
    rv_d,
    sh,
    shid,
    own_out,
    zr,
    tok_v,
    gain_v,
    ids_v,
    weights_v,
    sg_v,
    su_v,
    sd_v,
    gain_b,
    table_v,
    st_g,
    st_u,
    st_d,
    sb_g,
    sb_u,
    sb_d,
    tok,
    hid,
    xs,
    xr,
    zs,
    acc,
    load_sem,
    a2a_send,
    a2a_recv,
    tok_send,
    tok_recv,
    tok_tsend,
    tok_trecv,
    sh_send,
    sh_recv,
    hid_csend,
    hid_ysend,
    hid_fsend,
    hid_recv,
    shid_send,
    shid_recv,
    x_send,
    x_recv,
    z_send,
    z_recv,
):
    nx = 2
    me = lax.axis_index("fs")
    tp = lax.axis_index("tp")
    z, x = me // nx, me % nx
    partner = flip(tp, 1, ranks)
    across = flip(tp, 2, ranks)
    per = eg.shape[0] // groups
    experts = eg.shape[0]
    rows_w = eg.shape[1]
    rows_d = ed.shape[1]
    tok_count, features = tokens.shape
    share = tok_count // ranks
    hcols = eg.shape[2]
    dcols = ed.shape[2]
    hw = dcols // 2
    parts = ((0, hw), (hw, hw // 2), (hw + hw // 2, hw // 2))
    inn = ((z + 1) // 2) % 2
    inner, edge = inn == 1, inn == 0
    near, side, far_in, far_out = (flip(me, m, groups) for m in (2, 1, 6, 4))
    far = (inn * far_in + (1 - inn) * far_out, inn * far_out + (1 - inn) * far_in)

    pairs = (
        (gain, gain_v),
        (ids, ids_v),
        (weights, weights_v),
        (tokens, tok_v),
        (eg, st_g),
        (eu, st_u),
        (sg, sg_v),
        (su, su_v),
        (sd, sd_v),
        (ed, st_d),
    )
    loads = [pltpu.make_async_copy(a, b, load_sem.at[i]) for i, (a, b) in enumerate(pairs)]
    for load in loads:
        load.start()

    barrier = pltpu.get_barrier_semaphore()
    for o in range(1, groups):
        pl.semaphore_signal(
            barrier, inc=1, device_id={"fs": flip(me, o, groups)}, device_id_type=MESH
        )
    for o in range(1, ranks):
        pl.semaphore_signal(
            barrier, inc=1, device_id={"tp": flip(tp, o, ranks)}, device_id_type=MESH
        )

    def cast(stage, sendbuf, scaled, piece):
        @pl.loop(0, groups)
        def _(owner):
            e = owner * per + piece
            value = stage[e]
            if scaled:
                value = value * gain_b[...]
            sendbuf[e] = value.astype(jnp.bfloat16)

    mine = pl.ds(tp * share, share)
    theirs = pl.ds(across * share, share)

    def fs_copy(src, dst, send, recv, target):
        return pltpu.make_async_remote_copy(
            src_ref=src,
            dst_ref=dst,
            send_sem=send,
            recv_sem=recv,
            device_id={"fs": target},
            device_id_type=MESH,
        )

    def tp_copy(src, dst, send, recv, target):
        return pltpu.make_async_remote_copy(
            src_ref=src,
            dst_ref=dst,
            send_sem=send,
            recv_sem=recv,
            device_id={"tp": target},
            device_id_type=MESH,
        )

    ways = (near, side, far_in)

    def tok_copy(way, block):
        ref = tok.at[block, mine]
        return fs_copy(ref, ref, tok_send.at[way, block], tok_recv.at[block], ways[way])

    def sh_copy(way, block, part):
        ref = sh.at[block, part]
        return fs_copy(
            ref, ref, sh_send.at[way, block, part], sh_recv.at[block, part], ways[way]
        )

    def if_inner(act):
        pl.when(inner)(act)

    def tok_share(kind, block):
        rows = theirs if kind == 2 else mine
        return tp_copy(
            tok.at[block, rows],
            tok.at[block, rows],
            tok_tsend.at[kind, block],
            tok_trecv.at[kind, block],
            across if kind == 1 else partner,
        )

    def tok_arrive(block):
        tok_copy(0, block).wait_recv()
        tok_share(0, block).start()
        tok_share(1, block).start()

    def tok_moves(stage, act):
        if stage == 0:
            if_inner(lambda: act(tok_copy(2, me)))
            act(tok_copy(0, me))
            act(tok_copy(1, me))
        elif stage == 1:
            if_inner(lambda: act(tok_copy(2, near)))
            act(tok_copy(1, near))
        else:
            if_inner(lambda: act(tok_copy(0, far[stage - 2])))
            act(tok_copy(1, far[stage - 2]))

    def start(c):
        c.start()

    def wait_send(c):
        c.wait_send()

    order = (6, 7, 4, 5, 2, 3, 1)

    def a2a_ends(index, piece, owner_at, row_at):
        if index < 2:
            sendbuf, recvbuf = ((sb_g, rv_g), (sb_u, rv_u))[index]
            return (
                sendbuf.at[owner_at * per + piece],
                recvbuf.at[piece, pl.ds(row_at * rows_w, rows_w), :],
            )
        columns = pl.ds(*parts[piece])
        return (
            sb_d.at[pl.ds(owner_at * per, per), :, columns],
            rv_d.at[:, pl.ds(row_at * rows_d, rows_d), columns],
        )

    def a2a_copy(index, piece, o):
        target = flip(me, o, groups)
        src, dst = a2a_ends(index, piece, target, me)
        return fs_copy(
            src, dst, a2a_send.at[index, piece, o], a2a_recv.at[index, piece, o], target
        )

    def a2a_start(index, piece):
        for o in order:
            a2a_copy(index, piece, o).start()

    def a2a_own(index, piece):
        src, dst = a2a_ends(index, piece, me, me)
        dst[...] = src[...]

    def a2a_arrive(index, piece):
        for o in order:
            a2a_copy(index, piece, o).wait_recv()

    def far_start(index, piece):
        for o in order[:4]:
            a2a_copy(index, piece, o).start()

    def close_start(index, piece):
        for o in order[4:]:
            a2a_copy(index, piece, o).start()

    with scope("gain"):
        loads[0].wait()
        at_row = lax.broadcasted_iota(jnp.int32, (rows_w, rows_w), 0)
        at_column = lax.broadcasted_iota(jnp.int32, (rows_w, rows_w), 1)
        column = jnp.sum(
            jnp.where(at_row == at_column, gain_v[...], 0.0), axis=1, keepdims=True
        )
        gain_b[...] = jnp.broadcast_to(column, (rows_w, hcols))

    with scope("table"):
        loads[1].wait()
        loads[2].wait()
        row = lax.broadcasted_iota(jnp.int32, (experts, tok_count), 0)
        table = jnp.zeros((experts, tok_count), jnp.float32)
        for k in range(ids.shape[0]):
            table = table + jnp.where(row == ids_v[k : k + 1, :], weights_v[k : k + 1, :], 0.0)
        high = table.astype(jnp.bfloat16).astype(jnp.float32)
        middle = (table - high).astype(jnp.bfloat16).astype(jnp.float32)
        table_v[...] = jnp.zeros(table_v.shape, jnp.float32)
        for i, value in enumerate((high, middle, table - high - middle)):
            table_v[i * experts : (i + 1) * experts, 0:tok_count] = value
        tok[me, :, features : features + LANES] = table_v[...].T[0:tok_count].astype(jnp.bfloat16)

    def norm(first, count):
        @pl.loop(0, count // 16)
        def _(i):
            rows = pl.ds(first + i * 16, 16)
            wide = tok_v[rows, :].astype(jnp.float32)
            mean = jnp.mean(wide * wide, axis=-1, keepdims=True)
            tok[me, rows, 0:features] = (wide * lax.rsqrt(mean + EPS)).astype(jnp.bfloat16)

    with scope("norm"):
        loads[3].wait()
        norm(tp * share, share)

    with scope("barrier"):
        pl.semaphore_wait(barrier, groups + ranks - 2)

    with scope("launch"):
        tok_moves(0, start)
        loads[4].wait()
        cast(st_g, sb_g, True, 0)

        @pl.when(edge)
        def _():
            far_start(0, 0)

        close_start(0, 0)
        for o in range(1, ranks):
            norm(flip(tp, o, ranks) * share, share)
        loads[5].wait()
        cast(st_u, sb_u, True, 0)
    with scope("near_tokens"):
        tok_arrive(near)
        tok_moves(1, start)

        @pl.when(inner)
        def _():
            far_start(0, 0)

        far_start(1, 0)
        close_start(1, 0)
    with scope("casts"):
        for i in range(6, 10):
            loads[i].wait()
        sh[me, 0] = (sg_v[...] * gain_b[...]).astype(jnp.bfloat16)
        sh[me, 1] = (su_v[...] * gain_b[...]).astype(jnp.bfloat16)
        sh[me, 2, 0:rows_d] = sd_v[:, 0:hw].astype(jnp.bfloat16)
        sh[me, 2, rows_d : 2 * rows_d] = sd_v[:, hw:dcols].astype(jnp.bfloat16)
        for piece in range(1, per):
            cast(st_g, sb_g, True, piece)
            cast(st_u, sb_u, True, piece)
        for piece in range(per):
            cast(st_d, sb_d, False, piece)
        for index in range(2):
            for piece in range(per):
                a2a_own(index, piece)
        for piece in range(len(parts)):
            a2a_own(2, piece)
    with scope("far_tokens0"):
        tok_arrive(far[0])
        tok_moves(2, start)
    with scope("far_tokens1"):
        tok_arrive(far[1])
        tok_moves(3, start)
        for part in range(3):
            sh_copy(0, me, part).start()
            sh_copy(1, me, part).start()
        for part in range(2):
            if_inner(lambda: sh_copy(2, me, part).start())
    with scope("side_tokens"):
        for m in (1, 3, 5, 7):
            tok_arrive(flip(me, m, groups))
    with scope("near_shared"):
        for part in range(3):
            sh_copy(0, near, part).wait_recv()
            if part < 2:
                if_inner(lambda: sh_copy(2, near, part).start())
            sh_copy(1, near, part).start()
    with scope("arrive_g0"):
        a2a_arrive(0, 0)
        a2a_start(0, 1)
    with scope("shares"):
        for o in range(1, groups):
            tok_share(1, flip(me, o, groups)).wait_recv()
            tok_share(2, flip(me, o, groups)).start()
        for o in range(1, groups):
            tok_share(0, flip(me, o, groups)).wait_recv()
            tok_share(2, flip(me, o, groups)).wait_recv()

    def far_shared(k, part):
        sh_copy(0, far[k], part).wait_recv()
        if_inner(lambda: sh_copy(0, far[k], part).start())
        sh_copy(1, far[k], part).start()

    def far_shared_start(part):
        for block in (me, near):
            if_inner(lambda: sh_copy(2, block, part).start())

    def shared_sum(part, blocks):
        total = jnp.zeros((tok_count, hcols), jnp.float32)
        for block in blocks:
            columns = pl.ds(pl.multiple_of(block * rows_w, rows_w), rows_w)
            total = total + jnp.dot(
                tok[me, :, columns], sh[block, part], preferred_element_type=jnp.float32
            )
        return total

    def shid_copy(o):
        return tp_copy(
            shid.at[tp], shid.at[tp], shid_send.at[o], shid_recv.at[o], flip(tp, o, ranks)
        )

    def hid_core(e, block):
        return tp_copy(
            hid.at[tp, block, e],
            hid.at[tp, block, e],
            hid_csend.at[e, block],
            hid_recv.at[0, e, block],
            partner,
        )

    def hid_across(e, block):
        return tp_copy(
            hid.at[tp, block, e],
            hid.at[tp, block, e],
            hid_ysend.at[e, block],
            hid_recv.at[1, e, block],
            across,
        )

    def hid_forward(e, block):
        return tp_copy(
            hid.at[across, block, e],
            hid.at[across, block, e],
            hid_fsend.at[e, block],
            hid_recv.at[2, e, block],
            partner,
        )

    def turn(o):
        return (me + o) % groups

    for e in range(per):
        with scope(f"arrive_u{e}"):
            if e == 1:
                a2a_arrive(0, 1)
                a2a_start(2, 0)
            a2a_arrive(1, e)
            if e == 0:
                a2a_start(1, 1)
            else:
                a2a_start(2, 1)
                a2a_start(2, 2)
                far_shared_start(2)
        with scope(f"hidden{e}"):

            @pl.loop(0, groups)
            def _(o):
                block = turn(o + 1)
                rows = tok[block, :, 0:features]
                first = jnp.dot(rows, rv_g[e], preferred_element_type=jnp.float32)
                second = jnp.dot(rows, rv_u[e], preferred_element_type=jnp.float32)
                hid[tp, block, e] = (jax.nn.silu(first) * second).astype(jnp.bfloat16)

                @pl.when(o >= 1)
                def _():
                    before = turn(o)
                    hid_across(e, before).start()
                    hid_core(e, before).start()

            hid_across(e, me).start()
            hid_core(e, me).start()
        if e == 0:
            with scope("far_shared_gu"):
                for k in range(2):
                    for part in range(2):
                        far_shared(k, part)
        with scope(f"forward{e}"):

            @pl.loop(0, groups)
            def _(o):
                block = turn(o + 1)
                hid_across(e, block).wait_recv()
                hid_forward(e, block).start()

        if e == 0:
            with scope("side_shared_gu"):
                for part in range(2):
                    for m in (1, 3, 5, 7):
                        sh_copy(1, flip(me, m, groups), part).wait_recv()
            with scope("shared_hidden"):
                first, second = (shared_sum(part, range(groups)) for part in range(2))
                shid[tp] = (jax.nn.silu(first) * second).astype(jnp.bfloat16)
                for stage in range(4):
                    tok_moves(stage, wait_send)
                for o in range(1, groups):
                    for kind in range(3):
                        tok_share(kind, flip(me, o, groups)).wait_send()
                for o in range(1, ranks):
                    shid_copy(o).start()

    with scope("hid_wait"):

        @pl.loop(1, groups + 1)
        def _(o):
            block = turn(o)
            for e in range(per):
                hid_core(e, block).wait_recv()
                hid_forward(e, block).wait_recv()

        @pl.loop(0, groups)
        def _(o):
            for e in range(per):
                hid_core(e, o).wait_send()
                hid_across(e, o).wait_send()
                hid_forward(e, o).wait_send()

    lanes = lax.broadcasted_iota(jnp.int32, (tok_count, LANES), 1)

    def block_out(block, part):
        offset, wide = parts[part]
        table = tok[block, :, features : features + LANES].astype(jnp.float32)
        total = jnp.zeros((tok_count, wide), jnp.float32)
        for e in range(per):
            expert = me * per + e
            weight = jnp.sum(
                jnp.where(
                    (lanes == expert) | (lanes == expert + experts) | (lanes == expert + 2 * experts),
                    table,
                    0.0,
                ),
                axis=1,
                keepdims=True,
            )
            out = jnp.zeros((tok_count, wide), jnp.float32)
            for r in range(ranks):
                out = out + jnp.dot(
                    hid[r, block, e],
                    rv_d[e, r * hcols : (r + 1) * hcols, offset : offset + wide],
                    preferred_element_type=jnp.float32,
                )
            total = total + weight * out
        return total

    def dest(k):
        step = (k + 2 * inn) % 4
        half = z // 2
        away = 1 - step // 2
        chosen = half * (1 - away) + (1 - half) * away
        is_inner = (step % 2) * (1 - away) * inn + (1 - step % 2) * (1 - away) * (1 - inn) + (1 - step % 2) * away
        return chosen * (3 - is_inner) + (1 - chosen) * is_inner

    def x_copy(part, k):
        columns = pl.ds(*parts[part])
        return fs_copy(
            xs.at[k, :, columns], xr.at[k, :, columns], x_send.at[part, k], x_recv.at[part, k], side
        )

    def z_copy(part, k, slot, target):
        columns = pl.ds(*parts[part])
        return fs_copy(
            zs.at[k, :, columns],
            zr.at[slot, :, columns],
            z_send.at[part, k],
            z_recv.at[part, slot],
            target,
        )

    def x_stage(part):
        columns = pl.ds(*parts[part])

        @pl.loop(0, 4)
        def _(k):
            xs[k, :, columns] = block_out(dest(k) * nx + 1 - x, part).astype(jnp.bfloat16)

            @pl.when(k >= 1)
            def _():
                x_copy(part, k - 1).start()

    def z_stage(part):
        columns = pl.ds(*parts[part])

        @pl.loop(0, 4)
        def _(k):
            total = block_out(dest(k) * nx + x, part)

            @pl.when(k == 0)
            def _():
                x_copy(part, 3).start()

            x_copy(part, k).wait_recv()
            total = total + xr[k, :, columns].astype(jnp.float32)
            acc[k, :, columns] = total
            zs[k, :, columns] = total.astype(jnp.bfloat16)

            @pl.when((k >= 1) & edge)
            def _():
                z_copy(part, k - 1, k + 1, near).start()

            @pl.when((k == 1) & inner)
            def _():
                z_copy(part, 0, 4, near).start()

    def z_join(part):
        columns = pl.ds(*parts[part])

        @pl.when(inner)
        def _():
            for k in (2, 3):
                z_copy(part, k, k, near).wait_recv()
                zs[k, :, columns] = (
                    acc[k, :, columns] + zr[k, :, columns].astype(jnp.float32)
                ).astype(jnp.bfloat16)
            own_out[:, columns] = acc[1, :, columns]
            z_copy(part, 2, 5, far_in).start()
            z_copy(part, 3, 5, far_out).start()

        @pl.when(edge)
        def _():
            own_out[:, columns] = acc[3, :, columns]

    for part in range(len(parts)):
        with scope(f"arrive_d{part}"):
            a2a_arrive(2, part)
        with scope(f"x_stage{part}"):
            x_stage(part)
        with scope(f"z_stage{part}"):
            z_stage(part)
        if part == len(parts) - 1:
            with scope("far_shared_d0"):
                far_shared(0, 2)
        with scope(f"z_join{part}"):
            z_join(part)
    with scope("far_shared_d1"):
        far_shared(1, 2)
    with scope("side_shared_d"):
        for m in (1, 3, 5, 7):
            sh_copy(1, flip(me, m, groups), 2).wait_recv()
    with scope("drain"):
        for index in range(3):
            for piece in range(per if index < 2 else len(parts)):
                for o in order:
                    a2a_copy(index, piece, o).wait_send()
        for part in range(3):
            for way in range(2):
                sh_copy(way, me, part).wait_send()
            sh_copy(1, near, part).wait_send()
            for k in range(2):
                if_inner(lambda: sh_copy(0, far[k], part).wait_send())
                sh_copy(1, far[k], part).wait_send()
            for block in (me, near):
                if_inner(lambda: sh_copy(2, block, part).wait_send())
        for part in range(len(parts)):
            for k in range(4):
                x_copy(part, k).wait_send()
            for k in range(3):

                @pl.when(edge)
                def _():
                    z_copy(part, k, k + 2, near).wait_send()

            @pl.when(inner)
            def _():
                for k in (0, 2, 3):
                    z_copy(part, k, 4, near).wait_send()

    with scope("last"):
        for part in range(len(parts)):
            for slot in (4, 5):
                z_copy(part, 0, slot, near).wait_recv()
        for o in range(1, ranks):
            shid_copy(o).wait_recv()
            shid_copy(o).wait_send()


def finish_kernel(
    rv_g, rv_u, rv_d, sh, shid, own_out, zr, gate, up, down, sgate, sup, sdown, mixed, mixed_v, sems
):
    rows_d, hw = sdown.shape[1], sdown.shape[2] // 2
    groups, hcols = sh.shape[0], shid.shape[2]
    moves = [
        (rv_g, gate),
        (rv_u, up),
        (rv_d, down),
        (sh.at[:, 0], sgate),
        (sh.at[:, 1], sup),
        (sh.at[:, 2, pl.ds(0, rows_d)], sdown.at[:, :, pl.ds(0, hw)]),
        (sh.at[:, 2, pl.ds(rows_d, rows_d)], sdown.at[:, :, pl.ds(hw, hw)]),
    ]
    copies = [pltpu.make_async_copy(a, b, sems.at[i]) for i, (a, b) in enumerate(moves)]
    for copy in copies:
        copy.start()
    for part in range(2):
        columns = slice(part * hw, (part + 1) * hw)
        total = own_out[:, columns]
        for slot in (4, 5):
            total = total + zr[slot, :, columns].astype(jnp.float32)
        for block in range(groups):
            at = block * rows_d
            total = total + jnp.dot(
                shid[at // hcols, :, at % hcols : at % hcols + rows_d],
                sh[block, 2, part * rows_d : (part + 1) * rows_d],
                preferred_element_type=jnp.float32,
            )
        mixed_v[:, columns] = total.astype(jnp.bfloat16)
    last = pltpu.make_async_copy(mixed_v, mixed, sems.at[len(moves)])
    last.start()
    for copy in copies:
        copy.wait()
    last.wait()


def dense_body(
    tokens,
    norm_gain,
    expert_gate,
    expert_up,
    expert_down,
    shared_gate,
    shared_up,
    shared_down,
    expert_ids,
    route_weights,
):
    groups, ranks = lax.axis_size("fs"), lax.axis_size("tp")
    experts, rows_w, hcols = expert_gate.shape
    rows_d, dcols = expert_down.shape[1:]
    per = experts // groups
    tok_count, features = tokens.shape
    total = features + LANES
    bf, f32 = jnp.bfloat16, jnp.float32
    dma = pltpu.SemaphoreType.DMA
    any_space = pl.BlockSpec(memory_space=pl.ANY)
    vmem = pl.BlockSpec(memory_space=pltpu.VMEM)
    hidden = hcols * ranks
    wide_rows = -(-tok_count // LANES) * LANES
    made = pl.pallas_call(
        functools.partial(fused_kernel, groups, ranks),
        out_shape=(
            pltpu.VMEM((per, features, hcols), bf),
            pltpu.VMEM((per, features, hcols), bf),
            pltpu.VMEM((per, hidden, dcols), bf),
            pltpu.VMEM((groups, 3, rows_w, hcols), bf),
            pltpu.VMEM((ranks, tok_count, hcols), bf),
            pltpu.VMEM((tok_count, dcols), f32),
            pltpu.VMEM((6, tok_count, dcols), bf),
        ),
        in_specs=[any_space] * 10,
        out_specs=(vmem,) * 7,
        scratch_shapes=[
            pltpu.VMEM((tok_count, features), bf),
            pltpu.VMEM((1, rows_w), f32),
            pltpu.VMEM((TOP_K, tok_count), jnp.int32),
            pltpu.VMEM((TOP_K, tok_count), f32),
            pltpu.VMEM((rows_w, hcols), f32),
            pltpu.VMEM((rows_w, hcols), f32),
            pltpu.VMEM((rows_d, dcols), f32),
            pltpu.VMEM((rows_w, hcols), f32),
            pltpu.VMEM((LANES, wide_rows), f32),
            pltpu.VMEM((experts, rows_w, hcols), f32),
            pltpu.VMEM((experts, rows_w, hcols), f32),
            pltpu.VMEM((experts, rows_d, dcols), f32),
            pltpu.VMEM((experts, rows_w, hcols), bf),
            pltpu.VMEM((experts, rows_w, hcols), bf),
            pltpu.VMEM((experts, rows_d, dcols), bf),
            pltpu.VMEM((groups, tok_count, total), bf),
            pltpu.VMEM((ranks, groups, per, tok_count, hcols), bf),
            pltpu.VMEM((4, tok_count, dcols), bf),
            pltpu.VMEM((4, tok_count, dcols), bf),
            pltpu.VMEM((4, tok_count, dcols), bf),
            pltpu.VMEM((4, tok_count, dcols), f32),
            dma((10,)),
            dma((3, max(per, 3), groups)),
            dma((3, max(per, 3), groups)),
            dma((3, groups)),
            dma((groups,)),
            dma((3, groups)),
            dma((3, groups)),
            dma((3, groups, 3)),
            dma((groups, 3)),
            dma((per, groups)),
            dma((per, groups)),
            dma((per, groups)),
            dma((3, per, groups)),
            dma((ranks,)),
            dma((ranks,)),
            dma((3, 4)),
            dma((3, 4)),
            dma((3, 4)),
            dma((3, 6)),
        ],
        compiler_params=pltpu.CompilerParams(
            collective_id=0, has_side_effects=True, vmem_limit_bytes=VMEM_BYTES
        ),
    )(
        tokens,
        norm_gain[None, :],
        expert_ids.T,
        route_weights.T,
        expert_gate,
        expert_up,
        expert_down,
        shared_gate,
        shared_up,
        shared_down,
    )
    gate, up, down, sgate, sup, sdown, mixed = pl.pallas_call(
        finish_kernel,
        out_shape=tuple(
            jax.ShapeDtypeStruct(shape, bf)
            for shape in (
                (per, features, hcols),
                (per, features, hcols),
                (per, hidden, dcols),
                (groups, rows_w, hcols),
                (groups, rows_w, hcols),
                (groups, rows_d, dcols),
                (tok_count, dcols),
            )
        ),
        in_specs=[vmem] * 7,
        out_specs=(any_space,) * 7,
        scratch_shapes=[pltpu.VMEM((tok_count, dcols), bf), dma((8,))],
        compiler_params=pltpu.CompilerParams(vmem_limit_bytes=VMEM_BYTES // 4),
    )(*made)
    return (
        gate,
        up,
        down,
        sgate.reshape(features, hcols),
        sup.reshape(features, hcols),
        sdown.reshape(hidden, dcols),
        mixed,
    )


def expert_hidden(rows, gate_new, up_new):
    first = jnp.einsum("secn,enf->secf", rows, gate_new, preferred_element_type=jnp.float32)
    second = jnp.einsum("secn,enf->secf", rows, up_new, preferred_element_type=jnp.float32)
    return (jax.nn.silu(first) * second).astype(jnp.bfloat16)


def body(
    tokens,
    norm_gain,
    expert_gate,
    expert_up,
    expert_down,
    shared_gate,
    shared_up,
    shared_down,
    expert_ids,
    route_weights,
):
    groups = lax.axis_size("fs")
    experts = expert_gate.shape[0]
    per_group = experts // groups
    tok_count = tokens.shape[0]
    capacity = 2 * tok_count * TOP_K // experts
    ranks = lax.axis_size("tp")
    square = expert_down.shape[1] * expert_down.shape[2] == shared_gate.size
    if capacity >= tok_count and per_group >= 2 and groups == 8 and ranks == 4 and square:
        return dense_body(
            tokens,
            norm_gain,
            expert_gate,
            expert_up,
            expert_down,
            shared_gate,
            shared_up,
            shared_down,
            expert_ids,
            route_weights,
        )
    gate_local = (expert_gate * norm_gain[None, :, None]).astype(jnp.bfloat16)
    up_local = (expert_up * norm_gain[None, :, None]).astype(jnp.bfloat16)
    down_local = expert_down.astype(jnp.bfloat16)
    gate_local = gate_local.reshape((groups, per_group) + gate_local.shape[1:])
    up_local = up_local.reshape((groups, per_group) + up_local.shape[1:])
    down_local = down_local.reshape((groups, per_group) + down_local.shape[1:])
    shared_first_local = (shared_gate * norm_gain[:, None]).astype(jnp.bfloat16)
    shared_second_local = (shared_up * norm_gain[:, None]).astype(jnp.bfloat16)
    shared_third_local = shared_down.astype(jnp.bfloat16)
    gate_moved, up_moved, down_moved = (
        lax.all_to_all(gate_local, "fs", split_axis=0, concat_axis=2, tiled=True),
        lax.all_to_all(up_local, "fs", split_axis=0, concat_axis=2, tiled=True),
        lax.all_to_all(down_local, "fs", split_axis=0, concat_axis=2, tiled=True),
    )
    down_ready = down_moved[0]
    gate_ready = gate_moved[0]
    up_ready = up_moved[0]
    shared_gate_ready, shared_up_ready, shared_down_ready = (
        lax.all_gather(shared_first_local, "fs", axis=0, tiled=True),
        lax.all_gather(shared_second_local, "fs", axis=0, tiled=True),
        lax.all_gather(shared_third_local, "fs", axis=0, tiled=True),
    )
    wide = tokens.astype(jnp.float32)
    normed = (wide * lax.rsqrt(jnp.mean(wide * wide, axis=-1, keepdims=True) + EPS)).astype(
        jnp.bfloat16
    )
    chosen = expert_ids.reshape(-1)
    onehot = (chosen[:, None] == jnp.arange(experts, dtype=jnp.int32)[None, :]).astype(jnp.int32)
    ranks = jnp.sum(jnp.cumsum(onehot, axis=0) * onehot, axis=1) - 1
    owners = jnp.arange(tok_count * TOP_K, dtype=jnp.int32) // TOP_K
    slot_token = jnp.zeros((experts, capacity), jnp.int32).at[chosen, ranks].set(owners)
    outgoing = normed[slot_token.reshape(-1)].reshape(groups, per_group, capacity, normed.shape[1])
    share = capacity // lax.axis_size("tp")
    mine = lax.dynamic_slice_in_dim(outgoing, lax.axis_index("tp") * share, share, 2)
    arrived = lax.all_to_all(mine, "fs", split_axis=0, concat_axis=0, tiled=True)
    hidden = expert_hidden(lax.all_gather(arrived, "tp", axis=2, tiled=True), gate_ready, up_ready)
    shared_first = jnp.dot(normed, shared_gate_ready, preferred_element_type=jnp.float32)
    shared_second = jnp.dot(normed, shared_up_ready, preferred_element_type=jnp.float32)
    shared_hidden = (jax.nn.silu(shared_first) * shared_second).astype(jnp.bfloat16)[None, None]
    columns = down_ready.shape[2]
    routed_piece = lax.all_gather(hidden, "tp", axis=3, tiled=True)
    shared_piece = lax.all_gather(shared_hidden, "tp", axis=3, tiled=True)
    routed_total = jnp.einsum(
        "secf,efd->secd", routed_piece, down_ready, preferred_element_type=jnp.float32
    )
    shared_total = jnp.einsum(
        "abtf,fd->abtd", shared_piece, shared_down_ready, preferred_element_type=jnp.float32
    )
    returned = lax.all_to_all(
        routed_total.astype(jnp.bfloat16), "fs", split_axis=0, concat_axis=0, tiled=True
    )
    returned = returned.reshape(experts * capacity, columns)
    picked = (
        returned[chosen * capacity + ranks].astype(jnp.float32).reshape(tok_count, TOP_K, columns)
    )
    routed = jnp.sum(picked * route_weights[:, :, None], axis=1)
    mixed = (shared_total[0, 0] + routed).astype(jnp.bfloat16)
    return (
        gate_ready,
        up_ready,
        down_ready,
        shared_gate_ready,
        shared_up_ready,
        shared_down_ready,
        mixed,
    )


def solution(mesh):
    in_specs = (
        P("fs", None),
        P("fs"),
        P(None, "fs", "tp"),
        P(None, "fs", "tp"),
        P(None, "fs", "tp"),
        P("fs", "tp"),
        P("fs", "tp"),
        P("fs", "tp"),
        P("fs", None),
        P("fs", None),
    )
    out_specs = (
        P("fs", None, "tp"),
        P("fs", None, "tp"),
        P("fs", None, "tp"),
        P(None, "tp"),
        P(None, "tp"),
        P(None, "tp"),
        P("fs", "tp"),
    )
    return jax.shard_map(body, mesh=mesh, in_specs=in_specs, out_specs=out_specs, check_vma=False)
```

time: 215 us -> 203 us (0.944)
  local copies, waits for them, and re-layouts: 10.4 us -> 0 us
  other arithmetic: 2.42 us -> 0 us
    unnamed x9 -> x0, local copies, waits for them, and re-layouts: 7.55 us -> none
    pallas_call x0 -> x1, Pallas kernels: none -> 3.71 us  [dense_body(): pl.pallas_call(finish_kernel, out_shape=tuple((jax.ShapeDtypeStruct(shape...]
    pallas_call x1, Pallas kernels: 202 us -> 199 us  [dense_body(): pl.pallas_call(functools.partial(fused_kernel, groups, ranks), out_shape=...]
    reduce_sum x2 -> x0, other arithmetic: 2.19 us -> none  [the longest x1 1.44 us: dense_body(): jnp.mean(wide * wide, axis=-1, keepdims=True) + EPS]
where the time goes in v1:
time: 203 us
  Pallas kernels  202 us (100%)
    pallas_call x1, Pallas kernels, dense_body(): pl.pallas_call(functools.partial(fused_kernel, groups, ranks), out_shape=...  199 us

profile of v1, /device:TPU:0, one launch (start us, length us, event | category | flops | bytes accessed | tf_op | source)
XLA Modules:
  0.0 203.0 jit_solution(13087295338198921500)
XLA Ops:
  0.6 198.6 %shard_map.153 = (bf16[2,2048,256]{2,1,0:T(8,128)(2,1)S(1)}, bf16[2,2048,256]{2,1,0:T(8,128)(2,1)S(1)}, bf16[2,1024,512]{2,1,0:T(8,128)(2,1)S(1)}, bf16[8,3,256,...) custom-call(bf16[192,2048]{1,0:T(8,128)(2,1)} %tokens.1, ...), custom_call_target="tpu_custom_call" | custom-call | tf_op jit(solution)/shard_map/pallas_call | solution.py:716
  199.3 3.7 %shard_map.154 = (bf16[2,2048,256]{2,1,0:T(8,128)(2,1)}, bf16[2,2048,256]{2,1,0:T(8,128)(2,1)}, bf16[2,1024,512]{2,1,0:T(8,128)(2,1)}, bf16[8,256,256]{2,1,0:T(8...) custom-call(bf16[2,2048,256]{2,1,0:T(8,128)(2,1)S(1)} %get-tuple-element.21.rv_g, ...), custom_call_target="tpu_custom_call" | custom-call | tf_op jit(solution)/shard_map/pallas_call | solution.py:786

commit v2 on v1

--- a/solution.py
+++ b/solution.py
@@ -74,12 +74,12 @@
     tok_recv,
     tok_tsend,
     tok_trecv,
+    tok_yrecv,
     sh_send,
     sh_recv,
-    hid_csend,
-    hid_ysend,
-    hid_fsend,
+    hid_send,
     hid_recv,
+    hid_yrecv,
     shid_send,
     shid_recv,
     x_send,
@@ -170,12 +170,12 @@
 
     def tok_copy(way, block):
         ref = tok.at[block, mine]
-        return fs_copy(ref, ref, tok_send.at[way, block], tok_recv.at[block], ways[way])
+        return fs_copy(ref, ref, tok_send.at[way], tok_recv.at[block], ways[way])
 
     def sh_copy(way, block, part):
         ref = sh.at[block, part]
         return fs_copy(
-            ref, ref, sh_send.at[way, block, part], sh_recv.at[block, part], ways[way]
+            ref, ref, sh_send.at[way], sh_recv.at[block, part], ways[way]
         )
 
     def if_inner(act):
@@ -186,8 +186,8 @@
         return tp_copy(
             tok.at[block, rows],
             tok.at[block, rows],
-            tok_tsend.at[kind, block],
-            tok_trecv.at[kind, block],
+            tok_tsend.at[kind],
+            tok_yrecv.at[block] if kind == 1 else tok_trecv.at[kind // 2],
             across if kind == 1 else partner,
         )
 
@@ -233,28 +233,41 @@
         target = flip(me, o, groups)
         src, dst = a2a_ends(index, piece, target, me)
         return fs_copy(
-            src, dst, a2a_send.at[index, piece, o], a2a_recv.at[index, piece, o], target
+            src, dst, a2a_send.at[index], a2a_recv.at[index, piece], target
         )
 
     def a2a_start(index, piece):
-        for o in order:
-            a2a_copy(index, piece, o).start()
+        far_start(index, piece)
+        close_start(index, piece)
 
     def a2a_own(index, piece):
         src, dst = a2a_ends(index, piece, me, me)
         dst[...] = src[...]
 
+    def settle(ref, sem):
+        pltpu.make_async_copy(ref, ref, sem).wait()
+
     def a2a_arrive(index, piece):
-        for o in order:
-            a2a_copy(index, piece, o).wait_recv()
+        others = groups - 1
+        if index < 2:
+            ref = (rv_g, rv_u)[index].at[piece, pl.ds(0, others * rows_w)]
+        else:
+            ref = rv_d.at[:, pl.ds(0, others * rows_d), pl.ds(*parts[piece])]
+        settle(ref, a2a_recv.at[index, piece])
+
+    def if_edge(act):
+        pl.when(edge)(act)
+
+    def starts(index, piece, targets):
+        for o in targets:
+            a2a_copy(index, piece, o).start()
 
     def far_start(index, piece):
-        for o in order[:4]:
-            a2a_copy(index, piece, o).start()
+        if_inner(lambda: starts(index, piece, (4, 5, 6, 7)))
+        if_edge(lambda: starts(index, piece, (6, 7, 4, 5)))
 
     def close_start(index, piece):
-        for o in order[4:]:
-            a2a_copy(index, piece, o).start()
+        starts(index, piece, (2, 3, 1))
 
     with scope("gain"):
         loads[0].wait()
@@ -299,10 +312,7 @@
         loads[4].wait()
         cast(st_g, sb_g, True, 0)
 
-        @pl.when(edge)
-        def _():
-            far_start(0, 0)
-
+        if_edge(lambda: starts(0, 0, (6, 7, 4, 5)))
         close_start(0, 0)
         for o in range(1, ranks):
             norm(flip(tp, o, ranks) * share, share)
@@ -312,10 +322,7 @@
         tok_arrive(near)
         tok_moves(1, start)
 
-        @pl.when(inner)
-        def _():
-            far_start(0, 0)
-
+        if_inner(lambda: starts(0, 0, (4, 5, 6, 7)))
         far_start(1, 0)
         close_start(1, 0)
     with scope("casts"):
@@ -341,35 +348,32 @@
     with scope("far_tokens1"):
         tok_arrive(far[1])
         tok_moves(3, start)
-        for part in range(3):
-            sh_copy(0, me, part).start()
-            sh_copy(1, me, part).start()
-        for part in range(2):
-            if_inner(lambda: sh_copy(2, me, part).start())
     with scope("side_tokens"):
         for m in (1, 3, 5, 7):
             tok_arrive(flip(me, m, groups))
-    with scope("near_shared"):
+    with scope("arrive_g0"):
+        a2a_arrive(0, 0)
+        for part in range(3):
+            if_edge(lambda: sh_copy(0, me, part).start())
+        a2a_start(0, 1)
+    with scope("shares"):
+        for o in range(1, groups):
+            tok_share(1, flip(me, o, groups)).wait_recv()
+            tok_share(2, flip(me, o, groups)).start()
+        for i in range(2):
+            settle(tok.at[pl.ds(0, groups - 1), mine], tok_trecv.at[i])
+
+    def far_shared(k, part):
+        sh_copy(0, far[k], part).wait_recv()
+        if_inner(lambda: sh_copy(0, far[k], part).start())
+        sh_copy(1, far[k], part).start()
+
+    def near_shared():
         for part in range(3):
             sh_copy(0, near, part).wait_recv()
             if part < 2:
                 if_inner(lambda: sh_copy(2, near, part).start())
             sh_copy(1, near, part).start()
-    with scope("arrive_g0"):
-        a2a_arrive(0, 0)
-        a2a_start(0, 1)
-    with scope("shares"):
-        for o in range(1, groups):
-            tok_share(1, flip(me, o, groups)).wait_recv()
-            tok_share(2, flip(me, o, groups)).start()
-        for o in range(1, groups):
-            tok_share(0, flip(me, o, groups)).wait_recv()
-            tok_share(2, flip(me, o, groups)).wait_recv()
-
-    def far_shared(k, part):
-        sh_copy(0, far[k], part).wait_recv()
-        if_inner(lambda: sh_copy(0, far[k], part).start())
-        sh_copy(1, far[k], part).start()
 
     def far_shared_start(part):
         for block in (me, near):
@@ -393,8 +397,8 @@
         return tp_copy(
             hid.at[tp, block, e],
             hid.at[tp, block, e],
-            hid_csend.at[e, block],
-            hid_recv.at[0, e, block],
+            hid_send.at[0],
+            hid_recv,
             partner,
         )
 
@@ -402,8 +406,8 @@
         return tp_copy(
             hid.at[tp, block, e],
             hid.at[tp, block, e],
-            hid_ysend.at[e, block],
-            hid_recv.at[1, e, block],
+            hid_send.at[1],
+            hid_yrecv.at[e, block],
             across,
         )
 
@@ -411,8 +415,8 @@
         return tp_copy(
             hid.at[across, block, e],
             hid.at[across, block, e],
-            hid_fsend.at[e, block],
-            hid_recv.at[2, e, block],
+            hid_send.at[2],
+            hid_recv,
             partner,
         )
 
@@ -427,10 +431,15 @@
             a2a_arrive(1, e)
             if e == 0:
                 a2a_start(1, 1)
+                for part in range(3):
+                    if_inner(lambda: sh_copy(0, me, part).start())
+                    sh_copy(1, me, part).start()
+                for part in range(2):
+                    if_inner(lambda: sh_copy(2, me, part).start())
             else:
                 a2a_start(2, 1)
+                far_shared_start(2)
                 a2a_start(2, 2)
-                far_shared_start(2)
         with scope(f"hidden{e}"):
 
             @pl.loop(0, groups)
@@ -450,10 +459,8 @@
             hid_across(e, me).start()
             hid_core(e, me).start()
         if e == 0:
-            with scope("far_shared_gu"):
-                for k in range(2):
-                    for part in range(2):
-                        far_shared(k, part)
+            with scope("near_shared"):
+                if_inner(lambda: near_shared())
         with scope(f"forward{e}"):
 
             @pl.loop(0, groups)
@@ -463,36 +470,17 @@
                 hid_forward(e, block).start()
 
         if e == 0:
-            with scope("side_shared_gu"):
-                for part in range(2):
-                    for m in (1, 3, 5, 7):
-                        sh_copy(1, flip(me, m, groups), part).wait_recv()
-            with scope("shared_hidden"):
-                first, second = (shared_sum(part, range(groups)) for part in range(2))
-                shid[tp] = (jax.nn.silu(first) * second).astype(jnp.bfloat16)
-                for stage in range(4):
-                    tok_moves(stage, wait_send)
-                for o in range(1, groups):
-                    for kind in range(3):
-                        tok_share(kind, flip(me, o, groups)).wait_send()
-                for o in range(1, ranks):
-                    shid_copy(o).start()
+            with scope("edge_near_shared"):
+                if_edge(lambda: near_shared())
+            with scope("far_shared_gu"):
+                for k in range(2):
+                    for part in range(2):
+                        far_shared(k, part)
 
     with scope("hid_wait"):
-
-        @pl.loop(1, groups + 1)
-        def _(o):
-            block = turn(o)
-            for e in range(per):
-                hid_core(e, block).wait_recv()
-                hid_forward(e, block).wait_recv()
-
-        @pl.loop(0, groups)
-        def _(o):
-            for e in range(per):
-                hid_core(e, o).wait_send()
-                hid_across(e, o).wait_send()
-                hid_forward(e, o).wait_send()
+        settle(hid.at[pl.ds(0, 2)], hid_recv)
+        for kind in range(3):
+            settle(hid.at[tp], hid_send.at[kind])
 
     lanes = lax.broadcasted_iota(jnp.int32, (tok_count, LANES), 1)
 
@@ -532,7 +520,7 @@
     def x_copy(part, k):
         columns = pl.ds(*parts[part])
         return fs_copy(
-            xs.at[k, :, columns], xr.at[k, :, columns], x_send.at[part, k], x_recv.at[part, k], side
+            xs.at[k, :, columns], xr.at[k, :, columns], x_send, x_recv.at[part, k], side
         )
 
     def z_copy(part, k, slot, target):
@@ -540,32 +528,40 @@
         return fs_copy(
             zs.at[k, :, columns],
             zr.at[slot, :, columns],
-            z_send.at[part, k],
+            z_send,
             z_recv.at[part, slot],
             target,
         )
 
-    def x_stage(part):
+    def x_stage(part, pending):
         columns = pl.ds(*parts[part])
 
         @pl.loop(0, 4)
         def _(k):
             xs[k, :, columns] = block_out(dest(k) * nx + 1 - x, part).astype(jnp.bfloat16)
 
+            if pending is not None:
+
+                @pl.when(k == 0)
+                def _():
+                    x_copy(pending, 3).start()
+
             @pl.when(k >= 1)
             def _():
                 x_copy(part, k - 1).start()
 
-    def z_stage(part):
+    def z_stage(part, pending):
         columns = pl.ds(*parts[part])
 
         @pl.loop(0, 4)
         def _(k):
             total = block_out(dest(k) * nx + x, part)
 
-            @pl.when(k == 0)
-            def _():
-                x_copy(part, 3).start()
+            if pending is not None:
+
+                @pl.when(k == 0)
+                def _():
+                    x_copy(pending, 3).start()
 
             x_copy(part, k).wait_recv()
             total = total + xr[k, :, columns].astype(jnp.float32)
@@ -598,51 +594,64 @@
         def _():
             own_out[:, columns] = acc[3, :, columns]
 
-    for part in range(len(parts)):
+    def far_shared_d():
+        for k in range(2):
+            far_shared(k, 2)
+
+    def x_phase(part, pending):
         with scope(f"arrive_d{part}"):
             a2a_arrive(2, part)
         with scope(f"x_stage{part}"):
-            x_stage(part)
+            x_stage(part, pending)
+
+    def z_phase(part, pending):
         with scope(f"z_stage{part}"):
-            z_stage(part)
-        if part == len(parts) - 1:
-            with scope("far_shared_d0"):
-                far_shared(0, 2)
+            z_stage(part, pending)
+
+    def join_phase(part):
         with scope(f"z_join{part}"):
             z_join(part)
-    with scope("far_shared_d1"):
-        far_shared(1, 2)
+
+    x_phase(0, None)
+    x_phase(1, 0)
+    z_phase(0, 1)
+    with scope("side_shared_gu"):
+        for part in range(2):
+            for m in (1, 3, 5, 7):
+                sh_copy(1, flip(me, m, groups), part).wait_recv()
+    with scope("shared_hidden"):
+        first, second = (shared_sum(part, range(groups)) for part in range(2))
+        shid[tp] = (jax.nn.silu(first) * second).astype(jnp.bfloat16)
+        if_inner(lambda: settle(tok.at[pl.ds(0, 3), mine], tok_send.at[0]))
+        if_edge(lambda: settle(tok.at[pl.ds(0, 1), mine], tok_send.at[0]))
+        settle(tok.at[pl.ds(0, 4), mine], tok_send.at[1])
+        if_inner(lambda: settle(tok.at[pl.ds(0, 2), mine], tok_send.at[2]))
+        for kind in range(3):
+            settle(tok.at[pl.ds(0, groups - 1), mine], tok_tsend.at[kind])
+        for o in range(1, ranks):
+            shid_copy(o).start()
+    with scope("inner_far_shared_d"):
+        if_inner(lambda: far_shared_d())
+    x_phase(2, None)
+    join_phase(0)
+    z_phase(1, 2)
+    join_phase(1)
+    z_phase(2, None)
+    with scope("edge_far_shared_d"):
+        if_edge(lambda: far_shared_d())
+    join_phase(2)
     with scope("side_shared_d"):
         for m in (1, 3, 5, 7):
             sh_copy(1, flip(me, m, groups), 2).wait_recv()
     with scope("drain"):
-        for index in range(3):
-            for piece in range(per if index < 2 else len(parts)):
-                for o in order:
-                    a2a_copy(index, piece, o).wait_send()
-        for part in range(3):
-            for way in range(2):
-                sh_copy(way, me, part).wait_send()
-            sh_copy(1, near, part).wait_send()
-            for k in range(2):
-                if_inner(lambda: sh_copy(0, far[k], part).wait_send())
-                sh_copy(1, far[k], part).wait_send()
-            for block in (me, near):
-                if_inner(lambda: sh_copy(2, block, part).wait_send())
-        for part in range(len(parts)):
-            for k in range(4):
-                x_copy(part, k).wait_send()
-            for k in range(3):
-
-                @pl.when(edge)
-                def _():
-                    z_copy(part, k, k + 2, near).wait_send()
-
-            @pl.when(inner)
-            def _():
-                for k in (0, 2, 3):
-                    z_copy(part, k, 4, near).wait_send()
-
+        for index, sent in enumerate((sb_g, sb_u, sb_d)):
+            settle(sent.at[pl.ds(0, experts - per)], a2a_send.at[index])
+        if_inner(lambda: settle(sh.at[pl.ds(0, 3)], sh_send.at[0]))
+        if_edge(lambda: settle(sh.at[pl.ds(0, 1)], sh_send.at[0]))
+        settle(sh.at[pl.ds(0, 4)], sh_send.at[1])
+        if_inner(lambda: settle(sh.at[pl.ds(0, 2)], sh_send.at[2]))
+        settle(xs, x_send)
+        settle(zs.at[pl.ds(0, 3)], z_send)
     with scope("last"):
         for part in range(len(parts)):
             for slot in (4, 5):
@@ -749,23 +758,23 @@
             pltpu.VMEM((4, tok_count, dcols), bf),
             pltpu.VMEM((4, tok_count, dcols), f32),
             dma((10,)),
-            dma((3, max(per, 3), groups)),
-            dma((3, max(per, 3), groups)),
-            dma((3, groups)),
+            dma((3,)),
+            dma((3, max(per, 3))),
+            dma((3,)),
             dma((groups,)),
-            dma((3, groups)),
-            dma((3, groups)),
-            dma((3, groups, 3)),
+            dma((3,)),
+            dma((2,)),
+            dma((groups,)),
+            dma((3,)),
             dma((groups, 3)),
+            dma((3,)),
+            dma,
             dma((per, groups)),
-            dma((per, groups)),
-            dma((per, groups)),
-            dma((3, per, groups)),
             dma((ranks,)),
             dma((ranks,)),
+            dma,
             dma((3, 4)),
-            dma((3, 4)),
-            dma((3, 4)),
+            dma,
             dma((3, 6)),
         ],
         compiler_params=pltpu.CompilerParams(

time: 203 us -> 189 us (0.931)
  Pallas kernels: 202 us -> 188 us
    pallas_call x1, Pallas kernels: 199 us -> 184 us  [dense_body(): pl.pallas_call(functools.partial(fused_kernel, groups, ranks), out_shape=...]
where the time goes in v2:
time: 189 us; the launch traced here: 188 us
  Pallas kernels  188 us (99%)
    pallas_call x1, Pallas kernels, dense_body(): pl.pallas_call(functools.partial(fused_kernel, groups, ranks), out_shape=...  184 us

profile of v2, /device:TPU:0, one launch (start us, length us, event | category | flops | bytes accessed | tf_op | source)
XLA Modules:
  0.0 188.4 jit_solution(17286311135182845995)
XLA Ops:
  0.6 184.0 %shard_map.153 = (bf16[2,2048,256]{2,1,0:T(8,128)(2,1)S(1)}, bf16[2,2048,256]{2,1,0:T(8,128)(2,1)S(1)}, bf16[2,1024,512]{2,1,0:T(8,128)(2,1)S(1)}, bf16[8,3,256,...) custom-call(bf16[192,2048]{1,0:T(8,128)(2,1)} %tokens.1, ...), custom_call_target="tpu_custom_call" | custom-call | tf_op jit(solution)/shard_map/pallas_call | solution.py:725
  184.7 3.7 %shard_map.154 = (bf16[2,2048,256]{2,1,0:T(8,128)(2,1)}, bf16[2,2048,256]{2,1,0:T(8,128)(2,1)}, bf16[2,1024,512]{2,1,0:T(8,128)(2,1)}, bf16[8,256,256]{2,1,0:T(8...) custom-call(bf16[2,2048,256]{2,1,0:T(8,128)(2,1)S(1)} %get-tuple-element.21.rv_g, ...), custom_call_target="tpu_custom_call" | custom-call | tf_op jit(solution)/shard_map/pallas_call | solution.py:795

commit v3 on v2

--- a/solution.py
+++ b/solution.py
@@ -426,8 +426,13 @@
     for e in range(per):
         with scope(f"arrive_u{e}"):
             if e == 1:
-                a2a_arrive(0, 1)
-                a2a_start(2, 0)
+
+                @pl.when(edge)
+                def _():
+                    a2a_arrive(0, 1)
+                    starts(2, 0, (6, 7, 4, 5))
+
+                close_start(2, 0)
             a2a_arrive(1, e)
             if e == 0:
                 a2a_start(1, 1)
@@ -473,9 +478,15 @@
             with scope("edge_near_shared"):
                 if_edge(lambda: near_shared())
             with scope("far_shared_gu"):
-                for k in range(2):
-                    for part in range(2):
-                        far_shared(k, part)
+                for k, part in ((0, 0), (0, 1), (1, 0)):
+                    far_shared(k, part)
+
+                @pl.when(inner)
+                def _():
+                    a2a_arrive(0, 1)
+                    starts(2, 0, (4, 5, 6, 7))
+
+                far_shared(1, 1)
 
     with scope("hid_wait"):
         settle(hid.at[pl.ds(0, 2)], hid_recv)
@@ -632,11 +643,14 @@
             shid_copy(o).start()
     with scope("inner_far_shared_d"):
         if_inner(lambda: far_shared_d())
-    x_phase(2, None)
+    z_phase(1, None)
+    with scope("arrive_d2"):
+        a2a_arrive(2, 2)
     join_phase(0)
-    z_phase(1, 2)
     join_phase(1)
-    z_phase(2, None)
+    with scope("x_stage2"):
+        x_stage(2, None)
+    z_phase(2, 2)
     with scope("edge_far_shared_d"):
         if_edge(lambda: far_shared_d())
     join_phase(2)

time: 189 us -> 187 us (0.989)
  Pallas kernels: 188 us -> 186 us
where the time goes in v3:
time: 187 us
  Pallas kernels  186 us (99%)
    pallas_call x1, Pallas kernels, dense_body(): pl.pallas_call(functools.partial(fused_kernel, groups, ranks), out_shape=...  183 us

profile of v3, /device:TPU:0, one launch (start us, length us, event | category | flops | bytes accessed | tf_op | source)
XLA Modules:
  0.0 187.0 jit_solution(2869210648253327282)
XLA Ops:
  0.6 182.6 %shard_map.153 = (bf16[2,2048,256]{2,1,0:T(8,128)(2,1)S(1)}, bf16[2,2048,256]{2,1,0:T(8,128)(2,1)S(1)}, bf16[2,1024,512]{2,1,0:T(8,128)(2,1)S(1)}, bf16[8,3,256,...) custom-call(bf16[192,2048]{1,0:T(8,128)(2,1)} %tokens.1, ...), custom_call_target="tpu_custom_call" | custom-call | tf_op jit(solution)/shard_map/pallas_call | solution.py:739
  183.3 3.7 %shard_map.154 = (bf16[2,2048,256]{2,1,0:T(8,128)(2,1)}, bf16[2,2048,256]{2,1,0:T(8,128)(2,1)}, bf16[2,1024,512]{2,1,0:T(8,128)(2,1)}, bf16[8,256,256]{2,1,0:T(8...) custom-call(bf16[2,2048,256]{2,1,0:T(8,128)(2,1)S(1)} %get-tuple-element.21.rv_g, ...), custom_call_target="tpu_custom_call" | custom-call | tf_op jit(solution)/shard_map/pallas_call | solution.py:809

commit v4 on v3

--- a/solution.py
+++ b/solution.py
@@ -77,6 +77,7 @@
     tok_yrecv,
     sh_send,
     sh_recv,
+    sh_srecv,
     hid_send,
     hid_recv,
     hid_yrecv,
@@ -86,6 +87,7 @@
     x_recv,
     z_send,
     z_recv,
+    z_last,
 ):
     nx = 2
     me = lax.axis_index("fs")
@@ -175,7 +177,11 @@
     def sh_copy(way, block, part):
         ref = sh.at[block, part]
         return fs_copy(
-            ref, ref, sh_send.at[way], sh_recv.at[block, part], ways[way]
+            ref,
+            ref,
+            sh_send.at[way],
+            sh_srecv.at[part // 2] if way == 1 else sh_recv.at[block // nx, part],
+            ways[way],
         )
 
     def if_inner(act):
@@ -390,7 +396,7 @@
 
     def shid_copy(o):
         return tp_copy(
-            shid.at[tp], shid.at[tp], shid_send.at[o], shid_recv.at[o], flip(tp, o, ranks)
+            shid.at[tp], shid.at[tp], shid_send, shid_recv, flip(tp, o, ranks)
         )
 
     def hid_core(e, block):
@@ -521,11 +527,11 @@
         return total
 
     def dest(k):
-        step = (k + 2 * inn) % 4
         half = z // 2
-        away = 1 - step // 2
+        away = 1 - k // 2
         chosen = half * (1 - away) + (1 - half) * away
-        is_inner = (step % 2) * (1 - away) * inn + (1 - step % 2) * (1 - away) * (1 - inn) + (1 - step % 2) * away
+        own = (1 - k % 2) * (1 - inn) + (k % 2) * inn
+        is_inner = (1 - k % 2) * away + own * (1 - away)
         return chosen * (3 - is_inner) + (1 - chosen) * is_inner
 
     def x_copy(part, k):
@@ -534,13 +540,13 @@
             xs.at[k, :, columns], xr.at[k, :, columns], x_send, x_recv.at[part, k], side
         )
 
-    def z_copy(part, k, slot, target):
+    def z_copy(part, k, slot, target, joins=False):
         columns = pl.ds(*parts[part])
         return fs_copy(
             zs.at[k, :, columns],
             zr.at[slot, :, columns],
             z_send,
-            z_recv.at[part, slot],
+            z_recv.at[part, slot - 2] if joins else z_last,
             target,
         )
 
@@ -561,49 +567,54 @@
             def _():
                 x_copy(part, k - 1).start()
 
-    def z_stage(part, pending):
+    def z_stage(part, pending, low, high, deferred):
         columns = pl.ds(*parts[part])
 
-        @pl.loop(0, 4)
+        @pl.loop(low, high)
         def _(k):
             total = block_out(dest(k) * nx + x, part)
 
             if pending is not None:
 
-                @pl.when(k == 0)
+                @pl.when((k == 0) & inner if part == 2 else k == 0)
                 def _():
                     x_copy(pending, 3).start()
+
+            @pl.when((k >= 1) & (k < 3) & edge)
+            def _():
+                z_copy(part, k - 1, k + 1, near, True).start()
+
+            @pl.when(k == 3)
+            def _():
+                z_copy(part, 2, 4, near).start()
+
+            if deferred:
+
+                @pl.when((k == 2) & inner)
+                def _():
+                    z_copy(part, 1, 5, far_out).start()
 
             x_copy(part, k).wait_recv()
             total = total + xr[k, :, columns].astype(jnp.float32)
             acc[k, :, columns] = total
             zs[k, :, columns] = total.astype(jnp.bfloat16)
 
-            @pl.when((k >= 1) & edge)
-            def _():
-                z_copy(part, k - 1, k + 1, near).start()
-
-            @pl.when((k == 1) & inner)
-            def _():
-                z_copy(part, 0, 4, near).start()
-
-    def z_join(part):
+        if high == 4:
+            own_out[:, columns] = acc[3, :, columns]
+
+    def z_join(part, deferred):
         columns = pl.ds(*parts[part])
 
         @pl.when(inner)
         def _():
-            for k in (2, 3):
-                z_copy(part, k, k, near).wait_recv()
+            for k in range(2):
+                z_copy(part, k, k + 2, near, True).wait_recv()
                 zs[k, :, columns] = (
-                    acc[k, :, columns] + zr[k, :, columns].astype(jnp.float32)
+                    acc[k, :, columns] + zr[k + 2, :, columns].astype(jnp.float32)
                 ).astype(jnp.bfloat16)
-            own_out[:, columns] = acc[1, :, columns]
-            z_copy(part, 2, 5, far_in).start()
-            z_copy(part, 3, 5, far_out).start()
-
-        @pl.when(edge)
-        def _():
-            own_out[:, columns] = acc[3, :, columns]
+            z_copy(part, 0, 5, far_in).start()
+            if not deferred:
+                z_copy(part, 1, 5, far_out).start()
 
     def far_shared_d():
         for k in range(2):
@@ -615,21 +626,19 @@
         with scope(f"x_stage{part}"):
             x_stage(part, pending)
 
-    def z_phase(part, pending):
-        with scope(f"z_stage{part}"):
-            z_stage(part, pending)
-
-    def join_phase(part):
+    def z_phase(part, pending, low=0, high=4, deferred=False):
+        with scope(f"z_stage{part}_{low}"):
+            z_stage(part, pending, low, high, deferred)
+
+    def join_phase(part, deferred=False):
         with scope(f"z_join{part}"):
-            z_join(part)
+            z_join(part, deferred)
 
     x_phase(0, None)
     x_phase(1, 0)
     z_phase(0, 1)
     with scope("side_shared_gu"):
-        for part in range(2):
-            for m in (1, 3, 5, 7):
-                sh_copy(1, flip(me, m, groups), part).wait_recv()
+        settle(sh.at[pl.ds(0, 4), pl.ds(0, 2)], sh_srecv.at[0])
     with scope("shared_hidden"):
         first, second = (shared_sum(part, range(groups)) for part in range(2))
         shid[tp] = (jax.nn.silu(first) * second).astype(jnp.bfloat16)
@@ -647,16 +656,24 @@
     with scope("arrive_d2"):
         a2a_arrive(2, 2)
     join_phase(0)
-    join_phase(1)
     with scope("x_stage2"):
         x_stage(2, None)
-    z_phase(2, 2)
-    with scope("edge_far_shared_d"):
-        if_edge(lambda: far_shared_d())
-    join_phase(2)
+    join_phase(1)
+    with scope("edge_far_shared_d0"):
+
+        @pl.when(edge)
+        def _():
+            sh_copy(0, far[0], 2).wait_recv()
+            x_copy(2, 3).start()
+            sh_copy(1, far[0], 2).start()
+
+    z_phase(2, 2, 0, 2)
+    with scope("edge_far_shared_d1"):
+        if_edge(lambda: far_shared(1, 2))
+    join_phase(2, True)
+    z_phase(2, None, 2, 4, True)
     with scope("side_shared_d"):
-        for m in (1, 3, 5, 7):
-            sh_copy(1, flip(me, m, groups), 2).wait_recv()
+        settle(sh.at[pl.ds(0, 4), 2], sh_srecv.at[1])
     with scope("drain"):
         for index, sent in enumerate((sb_g, sb_u, sb_d)):
             settle(sent.at[pl.ds(0, experts - per)], a2a_send.at[index])
@@ -667,12 +684,9 @@
         settle(xs, x_send)
         settle(zs.at[pl.ds(0, 3)], z_send)
     with scope("last"):
-        for part in range(len(parts)):
-            for slot in (4, 5):
-                z_copy(part, 0, slot, near).wait_recv()
-        for o in range(1, ranks):
-            shid_copy(o).wait_recv()
-            shid_copy(o).wait_send()
+        settle(zr.at[pl.ds(4, 2)], z_last)
+        settle(shid.at[pl.ds(0, ranks - 1)], shid_recv)
+        settle(shid.at[pl.ds(0, ranks - 1)], shid_send)
 
 
 def finish_kernel(
@@ -780,16 +794,18 @@
             dma((2,)),
             dma((groups,)),
             dma((3,)),
-            dma((groups, 3)),
+            dma((groups // 2, 3)),
+            dma((2,)),
             dma((3,)),
             dma,
             dma((per, groups)),
-            dma((ranks,)),
-            dma((ranks,)),
+            dma,
+            dma,
             dma,
             dma((3, 4)),
             dma,
-            dma((3, 6)),
+            dma((3, 2)),
+            dma,
         ],
         compiler_params=pltpu.CompilerParams(
             collective_id=0, has_side_effects=True, vmem_limit_bytes=VMEM_BYTES

time: 187 us -> 187 us (level)
  no operation moved by 1% of the time
where the time goes in v4:
time: 187 us
  Pallas kernels  186 us (99%)
    pallas_call x1, Pallas kernels, dense_body(): pl.pallas_call(functools.partial(fused_kernel, groups, ranks), out_shape=...  183 us

profile of v4, /device:TPU:0, one launch (start us, length us, event | category | flops | bytes accessed | tf_op | source)
XLA Modules:
  0.0 187.1 jit_solution(13509389478536212472)
XLA Ops:
  0.6 182.7 %shard_map.153 = (bf16[2,2048,256]{2,1,0:T(8,128)(2,1)S(1)}, bf16[2,2048,256]{2,1,0:T(8,128)(2,1)S(1)}, bf16[2,1024,512]{2,1,0:T(8,128)(2,1)S(1)}, bf16[8,3,256,...) custom-call(bf16[192,2048]{1,0:T(8,128)(2,1)} %tokens.1, ...), custom_call_target="tpu_custom_call" | custom-call | tf_op jit(solution)/shard_map/pallas_call | solution.py:753
  183.4 3.7 %shard_map.154 = (bf16[2,2048,256]{2,1,0:T(8,128)(2,1)}, bf16[2,2048,256]{2,1,0:T(8,128)(2,1)}, bf16[2,1024,512]{2,1,0:T(8,128)(2,1)}, bf16[8,256,256]{2,1,0:T(8...) custom-call(bf16[2,2048,256]{2,1,0:T(8,128)(2,1)S(1)} %get-tuple-element.21.rv_g, ...), custom_call_target="tpu_custom_call" | custom-call | tf_op jit(solution)/shard_map/pallas_call | solution.py:825
